TPU v7x, 32 devices: a whole 2x2x4 slice. The times are simulated.
32 devices in a mesh: sp: 8 (over z, y), tp: 4 (over x, core).
Axes of the slice: x: 2, y: 2, z: 4, core: 2. Of those that a mesh axis runs over, the one named last changes fastest.
Arguments:
- queries: bfloat16 [4096, 1024], P('sp', 'tp'), may hold values from -200 to 200
- keys: bfloat16 [4096, 1024], P('sp', 'tp'), may hold values from -6 to 6
- values: bfloat16 [4096, 1024], P('sp', 'tp'), may hold values from -24 to 24
- cum_gate: float32 [4096, 8], P('sp', 'tp'), may hold values from -414 to 0, as said below
- residual: bfloat16 [4096, 2048], P(('sp', 'tp')), may hold values from -1.5 to 1.5
- w_out: bfloat16 [1024, 2048], replicated, may hold values from -0.1875 to 0.1875
- gain: float32 [2048], replicated, may hold values from 0.1 to 1.9
- w_up: bfloat16 [2048, 8192], P('sp', 'tp'), may hold values from -0.125 to 0.125
- w_down: bfloat16 [8192, 2048], P('tp', 'sp'), may hold values from -0.0625 to 0.0625
Outputs:
- output: bfloat16 [4096, 2048], P(('sp', 'tp'))
Inputs may be any that keep to these rules, and one draw needn't show every extreme that they name: Within each head, cum_gate never rises from one position to the next.
All inputs are finite; a program needn't handle non-finite values.
Results may differ from a plain program's by a relative error of at most 0.022.
Values may be sent and summed in bfloat16 or wider, within the bound.
A program may use at most 128 MiB of HBM per device.

v0:
```python
import math
import jax
import jax.numpy as jnp
from jax import lax
from jax.sharding import PartitionSpec as P


def per_device(queries, keys, values, cum_gate, residual, w_out, gain, w_up, w_down):
    tok_rows, width = queries.shape
    heads_here = cum_gate.shape[1]
    head_size = width // heads_here
    score_scale = head_size ** (-0.5)
    row_offset = lax.axis_index("sp") * tok_rows
    query_heads = queries.reshape(tok_rows, heads_here, head_size)
    query_pos = row_offset + jnp.arange(tok_rows, dtype=jnp.int32)
    all_gates = lax.all_gather(cum_gate, "sp", axis=0, tiled=True)
    initial = (
        jnp.full((tok_rows, heads_here), -1e30, jnp.float32),
        jnp.zeros((tok_rows, heads_here), jnp.float32),
        jnp.zeros((tok_rows, heads_here, head_size), jnp.float32),
    )
    carried = initial
    key_rows = lax.all_gather(keys, "sp", axis=0, tiled=True)
    value_rows = lax.all_gather(values, "sp", axis=0, tiled=True)
    row_count = key_rows.shape[0]
    span_rows = math.gcd(row_count, 2048)
    block_count = row_count // span_rows
    key_blocks = key_rows.reshape(block_count, span_rows, heads_here, head_size)
    value_blocks = value_rows.reshape(block_count, span_rows, heads_here, head_size)
    first_pos = jnp.arange(block_count, dtype=jnp.int32) * span_rows

    def absorb_block(running, packed):
        running_max, running_sum, accumulated = running
        key_blk, value_blk, block_start = packed
        gate_blk = lax.dynamic_slice_in_dim(all_gates, block_start, span_rows, 0)
        scores = jnp.einsum(
            "qhd,khd->qhk", query_heads, key_blk, preferred_element_type=jnp.float32
        )
        scores = scores * score_scale + cum_gate[:, :, None] - gate_blk.T[None, :, :]
        key_pos = block_start + jnp.arange(span_rows, dtype=jnp.int32)
        scores = jnp.where(key_pos[None, None, :] <= query_pos[:, None, None], scores, -1e30)
        new_max = jnp.maximum(running_max, jnp.max(scores, axis=-1))
        rescale = jnp.exp(running_max - new_max)
        weights = jnp.exp(scores - new_max[:, :, None])
        running_sum = running_sum * rescale + jnp.sum(weights, axis=-1)
        product = jnp.einsum(
            "qhk,khd->qhd",
            weights.astype(jnp.bfloat16),
            value_blk,
            preferred_element_type=jnp.float32,
        )
        accumulated = accumulated * rescale[:, :, None] + product
        return ((new_max, running_sum, accumulated), None)

    carried, _ = lax.scan(absorb_block, carried, (key_blocks, value_blocks, first_pos))
    running_max, running_sum, accumulated = carried
    attended = (accumulated / running_sum[:, :, None]).reshape(tok_rows, width).astype(jnp.bfloat16)
    mine = lax.all_to_all(attended, "tp", split_axis=0, concat_axis=1, tiled=True)
    projected = jnp.dot(mine, w_out, preferred_element_type=jnp.float32)
    residual_sum = residual.astype(jnp.float32) + projected
    mean_square = jnp.mean(residual_sum * residual_sum, axis=-1, keepdims=True)
    normed = (residual_sum * lax.rsqrt(mean_square + 1e-06) * gain).astype(jnp.bfloat16)
    normed_all = lax.all_gather(normed, "tp", axis=0, tiled=True)
    up_proj = jnp.dot(
        normed_all,
        lax.all_gather(w_up, "sp", axis=0, tiled=True),
        preferred_element_type=jnp.float32,
    )
    hidden = jnp.square(jax.nn.relu(up_proj)).astype(jnp.bfloat16)
    down_whole = lax.all_gather(w_down, "sp", axis=1, tiled=True)
    rounded = jnp.dot(hidden, down_whole, preferred_element_type=jnp.float32).astype(jnp.bfloat16)
    branch_out = lax.psum_scatter(
        lax.optimization_barrier(rounded).astype(jnp.float32).astype(jnp.bfloat16),
        "tp",
        scatter_dimension=0,
        tiled=True,
    ).astype(jnp.float32)
    return (residual_sum + branch_out).astype(jnp.bfloat16)


def solution(mesh):
    return jax.shard_map(
        per_device,
        mesh=mesh,
        in_specs=(
            P("sp", "tp"),
            P("sp", "tp"),
            P("sp", "tp"),
            P("sp", "tp"),
            P(("sp", "tp"), None),
            P(),
            P(),
            P("sp", "tp"),
            P("tp", "sp"),
        ),
        out_specs=P(("sp", "tp"), None),
        check_vma=False,
    )
```

profile of v0, /device:TPU:0, one launch (start us, length us, event | category | flops | bytes accessed | tf_op | source)
XLA Modules:
  0.0 501.9 jit_solution(15590965651173478988)
XLA Ops:
  6.5 0.7 all-gather.6.cloned.1.call-update
  7.3 0.7 all-gather.8.cloned.1.call-update
  8.1 1.1 copy.17
  9.4 32.7 %all_gather.19 = f32[4096,2]{0,1:T(2,128)S(1)} all-gather(f32[512,2]{0,1:T(2,128)} %param.14), channel_id=1, replica_groups=mesh['sp'=8,'tp'=4] {'sp'}, dimensions={0}, use_global_device_ids=true | all-gather | bytes 36864 | tf_op jit(solution)/shard_map/all_gather | solution.py:16
  42.0 19.4 %all-gather.6.cloned.1.call-done = bf16[4096,256]{1,0:T(8,128)(2,1)} async-done(((bf16[512,256]{1,0:T(8,128)(2,1)}), bf16[4096,256]{1,0:T(8,128)(2,1)}) %all-gather.6.cloned.1.call-update) | async-done | bytes 2097168 | tf_op jit(solution)/shard_map/all_gather | solution.py:23
  61.4 4.0 reshape.62
  65.4 45.8 %all-gather.8.cloned.1.call-done = bf16[4096,256]{1,0:T(8,128)(2,1)} async-done(((bf16[512,256]{1,0:T(8,128)(2,1)}), bf16[4096,256]{1,0:T(8,128)(2,1)}) %all-gather.8.cloned.1.call-update) | async-done | bytes 2097168 | tf_op jit(solution)/shard_map/all_gather | solution.py:24
  111.2 4.0 reshape.64
  115.2 45.9 %while.15 = (s32[]{:T(128)}, f32[512,2]{0,1:T(2,128)S(1)}, f32[512,2]{0,1:T(2,128)S(1)}, f32[512,2,128]{0,2,1:T(8,128)}, s32[2]{0:T(128)S(1)}, /*index=5*/bf16[2...) while((s32[]{:T(128)}, f32[512,2]{0,1:T(2,128)S(1)}, ...), condition=%wide.region_3.4_spmd.clone, body=%wide.region_0.3_spmd.clone.sunk | while | flops 1110842880 | bytes 39239884 | solution.py:55
  115.2 0.6 dynamic_slice.26
  118.1 0.8 broadcast_compare_fusion.2
  118.9 2.7 constant_dynamic-slice_fusion.3
  121.6 4.6 fusion.40
  126.2 4.8 fusion.42
  131.0 0.8 copy.34
  131.8 6.2 %fusion.44 = f32[512,2,128]{0,2,1:T(8,128)} fusion(f32[2,2048,512]{2,1,0:T(8,128)} %get-tuple-element.231, f32[512,2]{0,1:T(2,128)S(1)} %fusion.41, f32[2,2048]{1,0:T(2,128)S(1)} %dynamic-slice_bitcast_fusion.2, f32[512,2]{0,1:T(2,128)S(1)} %get-tuple-element.270, pred[512,2048]{0,1:T(8,128)(4,1)S(1)} %broadcast_compare_fusion.2, ...), kind=kOutput, calls=%fused_computation.12.clone.1 | convolution fusion | flops 549847040 | bytes 11563009 | tf_op jit(solution)/shard_map/while/body/eval_jaxpr/qhk,khd->qhd/dot_general | solution.py:46
  141.0 0.8 broadcast_compare_fusion.2
  141.8 2.7 constant_dynamic-slice_fusion.3
  144.5 4.6 fusion.40
  149.1 4.8 fusion.42
  153.9 0.8 copy.34
  154.7 6.4 %fusion.44 = f32[512,2,128]{0,2,1:T(8,128)} fusion(f32[2,2048,512]{2,1,0:T(8,128)} %get-tuple-element.231, f32[512,2]{0,1:T(2,128)S(1)} %fusion.41, f32[2,2048]{1,0:T(2,128)S(1)} %dynamic-slice_bitcast_fusion.2, f32[512,2]{0,1:T(2,128)S(1)} %get-tuple-element.270, pred[512,2048]{0,1:T(8,128)(4,1)S(1)} %broadcast_compare_fusion.2, ...), kind=kOutput, calls=%fused_computation.12.clone.1 | convolution fusion | flops 549847040 | bytes 11563009 | tf_op jit(solution)/shard_map/while/body/eval_jaxpr/qhk,khd->qhd/dot_general | solution.py:46
  161.1 1.1 divide_convert_fusion
  162.4 8.5 %all_to_all.16 = bf16[4,128,256]{2,1,0:T(8,128)(2,1)S(1)} all-to-all(bf16[4,128,256]{2,1,0:T(8,128)(2,1)S(1)} %copy.24), channel_id=1, replica_groups=mesh['sp'=8,'tp'=4] {'tp'}, dimensions={0} | all-to-all | bytes 524288 | tf_op jit(solution)/shard_map/all_to_all | solution.py:58
  171.1 3.1 multiply_reduce_fusion
  174.3 0.9 multiply_convert_fusion.1
  176.7 19.0 %all-gather.10.cloned.1.call-done = bf16[512,2048]{1,0:T(8,128)(2,1)} async-done(((bf16[128,2048]{1,0:T(8,128)(2,1)}), bf16[512,2048]{1,0:T(8,128)(2,1)}) %all-gather.10.cloned.1.call-update) | async-done | bytes 2097168 | tf_op jit(solution)/shard_map/all_gather | solution.py:63
  195.6 126.5 %all-gather.12.cloned.1.call-done = bf16[2048,2048]{1,0:T(8,128)(2,1)} async-done(((bf16[256,2048]{1,0:T(8,128)(2,1)}), bf16[2048,2048]{1,0:T(8,128)(2,1)}) %all-gather.12.cloned.1.call-update) | async-done | bytes 8388624 | tf_op jit(solution)/shard_map/all_gather | solution.py:66
  322.1 125.0 %all-gather.14.cloned.1.call-done = bf16[2048,2048]{1,0:T(8,128)(2,1)} async-done(((bf16[2048,256]{1,0:T(8,128)(2,1)}), bf16[2048,2048]{1,0:T(8,128)(2,1)}) %all-gather.14.cloned.1.call-update) | async-done | bytes 8388624 | tf_op jit(solution)/shard_map/all_gather | solution.py:70
  447.1 16.5 %convolution_convert_fusion = bf16[512,2048]{1,0:T(8,128)(2,1)} fusion(bf16[2048,2048]{1,0:T(8,128)(2,1)} %all-gather.14.cloned.1.call-done, bf16[512,2048]{1,0:T(8,128)(2,1)} %all-gather.10.cloned.1.call-done, bf16[2048,2048]{1,0:T(8,128)(2,1)} %all-gather.12.cloned.1.call-done), kind=kOutput, calls=%fused_computation.30 | convolution fusion | flops 8594128896 | bytes 20971520 | tf_op jit(solution)/shard_map/dot_general | solution.py:71
  463.7 29.5 %reduce-scatter.2.cloned.1.call-done = bf16[128,2048]{1,0:T(8,128)(2,1)} async-done(((bf16[512,2048]{1,0:T(8,128)(2,1)}), bf16[128,2048]{1,0:T(8,128)(2,1)}) %reduce-scatter.2.cloned.1.call-update) | async-done | bytes 524304 | tf_op jit(solution)/shard_map/reduce_scatter | solution.py:72
  493.2 1.9 add_convert_fusion
  (36 shorter events, 4.0 us)
Async XLA Ops:
  6.5 108.6 %copy-start = (f32[512,2]{0,1:T(2,128)S(1)}, f32[512,2]{0,1:T(2,128)}, u32[]{:S(2)}) copy-start(f32[512,2]{0,1:T(2,128)} %param.14) | copy-start | bytes 12292
  6.5 54.9 %all-gather.6.cloned.1.call-start = ((), (), s32[]{:S(2)}) async-start(), calls=%async_computation.2 | async-start | bytes 2359296 | tf_op jit(solution)/shard_map/all_gather | solution.py:23
  7.3 103.9 %all-gather.8.cloned.1.call-start = ((), (), s32[]{:S(2)}) async-start(), calls=%async_computation.3 | async-start | bytes 2359296 | tf_op jit(solution)/shard_map/all_gather | solution.py:24
  8.0 187.6 %all-gather.10.cloned.1.call-start = ((), (), s32[]{:S(2)}) async-start(), calls=%async_computation.4 | async-start | bytes 2621440 | tf_op jit(solution)/shard_map/all_gather | solution.py:63
  161.1 13.2 %copy-start.1 = (f32[2048]{0:T(1024)S(1)}, f32[2048]{0:T(1024)}, u32[]{:S(2)}) copy-start(f32[2048]{0:T(1024)} %param.17) | copy-start | bytes 24580
  175.3 146.8 %all-gather.12.cloned.1.call-start = ((), (), s32[]{:S(2)}) async-start(), calls=%async_computation.5 | async-start | bytes 9437184 | tf_op jit(solution)/shard_map/all_gather | solution.py:66
  175.8 271.3 %all-gather.14.cloned.1.call-start = ((), (), s32[]{:S(2)}) async-start(), calls=%async_computation.6 | async-start | bytes 9437184 | tf_op jit(solution)/shard_map/all_gather | solution.py:70
  176.4 316.7 %reduce-scatter.2.cloned.1.call-start = ((), (), s32[]{:S(2)}) async-start(), calls=%async_computation.7 | async-start | bytes 2621440 | tf_op jit(solution)/shard_map/reduce_scatter | solution.py:72
Sparse Core Ops, SparseCore 0:
  9.5 51.9 all-gather.5
  63.5 47.6 all-gather.7
  175.4 20.1 all-gather.9
  197.6 124.4 all-gather.11
  324.0 123.1 all-gather.13
  463.8 29.3 reduce-scatter.1
where the time goes:
time: 502 us
  waiting for transfers between devices  368 us (73%)
  matrix products  41.4 us (8%)
  blocking collectives  41.2 us (8%)
  local copies, waits for them, and re-layouts  18 us (4%)
  other arithmetic  16.3 us (3%)
  between operations  13.6 us (3%)
    all_gather x1, waiting for transfers between devices, per_device(): lax.all_gather(w_up, 'sp', axis=0, tiled=True)  126 us
    all_gather x1, waiting for transfers between devices, per_device(): down_whole = lax.all_gather(w_down, 'sp', axis=1, tiled=True)  125 us
    all_gather x1, waiting for transfers between devices, per_device(): value_rows = lax.all_gather(values, 'sp', axis=0, tiled=True)  45.8 us
    all_gather x1, blocking collectives, per_device(): all_gates = lax.all_gather(cum_gate, 'sp', axis=0, tiled=True)  32.7 us
    reduce_scatter x1, waiting for transfers between devices, per_device(): lax.psum_scatter(lax.optimization_barrier(rounded).astype(jnp.float32).as...  29.5 us
    all_gather x1, waiting for transfers between devices, per_device(): key_rows = lax.all_gather(keys, 'sp', axis=0, tiled=True)  19.4 us
    all_gather x1, waiting for transfers between devices, per_device(): normed_all = lax.all_gather(normed, 'tp', axis=0, tiled=True)  19 us
    dot_general x1, matrix products, per_device(): jnp.dot(hidden, down_whole, preferred_element_type=jnp.float32)  16.5 us
  transfers between devices with their start and end apart: 6, of which 6 were waited for; matrix products, arithmetic and copies ran while one was open for 1% of the time, Pallas kernels for 0%

commit v1 on v0

--- a/solution.py
+++ b/solution.py
@@ -67,7 +67,7 @@
         preferred_element_type=jnp.float32,
     )
     hidden = jnp.square(jax.nn.relu(up_proj)).astype(jnp.bfloat16)
-    down_whole = lax.all_gather(w_down, "sp", axis=1, tiled=True)
+    down_whole = jnp.concatenate(lax.all_gather(w_down, "sp"), axis=1)
     rounded = jnp.dot(hidden, down_whole, preferred_element_type=jnp.float32).astype(jnp.bfloat16)
     branch_out = lax.psum_scatter(
         lax.optimization_barrier(rounded).astype(jnp.float32).astype(jnp.bfloat16),

time: 502 us -> 441 us (0.88)
  waiting for transfers between devices: 368 us -> 293 us
  local copies, waits for them, and re-layouts: 18 us -> 29.8 us
    all_gather x1, waiting for transfers between devices: 125 us -> 59.6 us  [per_device(): down_whole = jnp.concatenate(lax.all_gather(w_down, 'sp'), axis=1)]
    reshape x0 -> x1, local copies, waits for them, and re-layouts: none -> 11.6 us  [per_device(): down_whole = jnp.concatenate(lax.all_gather(w_down, 'sp'), axis=1)]
    all_gather x1, waiting for transfers between devices: 19 us -> 10.6 us  [per_device(): normed_all = lax.all_gather(normed, 'tp', axis=0, tiled=True)]
  transfers between devices with their start and end apart: 6 -> 6, of which waited for: 6 -> 6; matrix products, arithmetic and copies ran while one was open for 1% -> 16% of each run, Pallas kernels for 0% -> 0%
where the time goes in v1:
time: 441 us; the launch traced here: 440 us
  waiting for transfers between devices  293 us (66%)
  matrix products  41.4 us (9%)
  blocking collectives  41.2 us (9%)
  local copies, waits for them, and re-layouts  29.8 us (7%)
  other arithmetic  16.4 us (4%)
  between operations  13.6 us (3%)
    all_gather x1, waiting for transfers between devices, per_device(): lax.all_gather(w_up, 'sp', axis=0, tiled=True)  126 us
    all_gather x1, waiting for transfers between devices, per_device(): down_whole = jnp.concatenate(lax.all_gather(w_down, 'sp'), axis=1)  59.6 us
    all_gather x1, waiting for transfers between devices, per_device(): value_rows = lax.all_gather(values, 'sp', axis=0, tiled=True)  45.8 us
    all_gather x1, blocking collectives, per_device(): all_gates = lax.all_gather(cum_gate, 'sp', axis=0, tiled=True)  32.7 us
    reduce_scatter x1, waiting for transfers between devices, per_device(): lax.psum_scatter(lax.optimization_barrier(rounded).astype(jnp.float32).as...  29.5 us
    all_gather x1, waiting for transfers between devices, per_device(): key_rows = lax.all_gather(keys, 'sp', axis=0, tiled=True)  18.6 us
    dot_general x1, matrix products, per_device(): jnp.dot(hidden, down_whole, preferred_element_type=jnp.float32)  16.5 us
    dot_general x2, matrix products, absorb_block(): jnp.einsum('qhk,khd->qhd', weights.astype(jnp.bfloat16), value_blk, prefe...  12.6 us
  transfers between devices with their start and end apart: 6, of which 6 were waited for; matrix products, arithmetic and copies ran while one was open for 16% of the time, Pallas kernels for 0%

profile of v1, /device:TPU:0, one launch (start us, length us, event | category | flops | bytes accessed | tf_op | source)
XLA Modules:
  0.0 439.9 jit_solution(5681036742826392756)
XLA Ops:
  6.5 0.7 all-gather.7.cloned.1.call-update
  7.3 0.7 all-gather.9.cloned.1.call-update
  8.8 1.1 copy.17
  10.1 32.7 %all_gather.22 = f32[4096,2]{0,1:T(2,128)S(1)} all-gather(f32[512,2]{0,1:T(2,128)} %param.14), channel_id=1, replica_groups=mesh['sp'=8,'tp'=4] {'sp'}, dimensions={0}, use_global_device_ids=true | all-gather | bytes 36864 | tf_op jit(solution)/shard_map/all_gather | solution.py:16
  42.8 18.6 %all-gather.7.cloned.1.call-done = bf16[4096,256]{1,0:T(8,128)(2,1)} async-done(((bf16[512,256]{1,0:T(8,128)(2,1)}), bf16[4096,256]{1,0:T(8,128)(2,1)}) %all-gather.7.cloned.1.call-update) | async-done | bytes 2097168 | tf_op jit(solution)/shard_map/all_gather | solution.py:23
  61.4 4.0 reshape.68
  65.4 45.8 %all-gather.9.cloned.1.call-done = bf16[4096,256]{1,0:T(8,128)(2,1)} async-done(((bf16[512,256]{1,0:T(8,128)(2,1)}), bf16[4096,256]{1,0:T(8,128)(2,1)}) %all-gather.9.cloned.1.call-update) | async-done | bytes 2097168 | tf_op jit(solution)/shard_map/all_gather | solution.py:24
  111.2 4.0 reshape.70
  115.1 46.6 %while.15 = (s32[]{:T(128)}, f32[512,2]{0,1:T(2,128)S(1)}, f32[512,2]{0,1:T(2,128)S(1)}, f32[512,2,128]{0,2,1:T(8,128)}, s32[2]{0:T(128)S(1)}, /*index=5*/bf16[2...) while((s32[]{:T(128)}, f32[512,2]{0,1:T(2,128)S(1)}, ...), condition=%wide.region_3.4_spmd.clone, body=%wide.region_0.3_spmd.clone.sunk | while | flops 1110842880 | bytes 39239884 | solution.py:55
  118.4 0.8 broadcast_compare_fusion.2
  119.2 2.8 constant_dynamic-slice_fusion.3
  122.0 4.5 %fusion.40 = (f32[512,2]{0,1:T(2,128)S(1)}, f32[2,2048,512]{2,1,0:T(8,128)}) fusion(f32[2,2048]{1,0:T(2,128)S(1)} %dynamic-slice_bitcast_fusion.2, f32[512,2]{0,1:T(2,128)S(1)} %get-tuple-element.270, pred[512,2048]{0,1:T(8,128)(4,1)S(1)} %broadcast_compare_fusion.2, bf16[512,2,128]{2,0,1:T(8,128)(2,1)S(1)} %get-tuple-element.269, ...), kind=kOutput, calls=%fused_computation.7.clone.1 | convolution fusion | flops 547355648 | bytes 10772480 | tf_op jit(solution)/shard_map/while/body/eval_jaxpr/qhd,khd->qhk/dot_general | solution.py:36
  126.6 4.8 %fusion.42 = f32[512,2]{0,1:T(2,128)S(1)} fusion(f32[2,2048,512]{2,1,0:T(8,128)} %get-tuple-element.231, f32[512,2]{0,1:T(2,128)S(1)} %fusion.41, f32[2,2048]{1,0:T(2,128)S(1)} %dynamic-slice_bitcast_fusion.2, f32[512,2]{0,1:T(2,128)S(1)} %get-tuple-element.270, pred[512,2048]{0,1:T(8,128)(4,1)S(1)} %broadcast_compare_fusion.2), kind=kLoop, calls=%fused_computation.6.clone.1 | loop fusion | flops 12581888 | bytes 9465856 | tf_op jit(solution)/shard_map/while/body/eval_jaxpr/reduce_sum | solution.py:45
  131.4 0.8 copy.35
  132.2 6.3 %fusion.44 = f32[512,2,128]{0,2,1:T(8,128)} fusion(f32[2,2048,512]{2,1,0:T(8,128)} %get-tuple-element.231, f32[512,2]{0,1:T(2,128)S(1)} %fusion.41, f32[2,2048]{1,0:T(2,128)S(1)} %dynamic-slice_bitcast_fusion.2, f32[512,2]{0,1:T(2,128)S(1)} %get-tuple-element.270, pred[512,2048]{0,1:T(8,128)(4,1)S(1)} %broadcast_compare_fusion.2, ...), kind=kOutput, calls=%fused_computation.12.clone.1 | convolution fusion | flops 549847040 | bytes 11563009 | tf_op jit(solution)/shard_map/while/body/eval_jaxpr/qhk,khd->qhd/dot_general | solution.py:46
  141.7 0.8 broadcast_compare_fusion.2
  142.5 2.7 constant_dynamic-slice_fusion.3
  145.2 4.6 %fusion.40 = (f32[512,2]{0,1:T(2,128)S(1)}, f32[2,2048,512]{2,1,0:T(8,128)}) fusion(f32[2,2048]{1,0:T(2,128)S(1)} %dynamic-slice_bitcast_fusion.2, f32[512,2]{0,1:T(2,128)S(1)} %get-tuple-element.270, pred[512,2048]{0,1:T(8,128)(4,1)S(1)} %broadcast_compare_fusion.2, bf16[512,2,128]{2,0,1:T(8,128)(2,1)S(1)} %get-tuple-element.269, ...), kind=kOutput, calls=%fused_computation.7.clone.1 | convolution fusion | flops 547355648 | bytes 10772480 | tf_op jit(solution)/shard_map/while/body/eval_jaxpr/qhd,khd->qhk/dot_general | solution.py:36
  149.8 4.8 %fusion.42 = f32[512,2]{0,1:T(2,128)S(1)} fusion(f32[2,2048,512]{2,1,0:T(8,128)} %get-tuple-element.231, f32[512,2]{0,1:T(2,128)S(1)} %fusion.41, f32[2,2048]{1,0:T(2,128)S(1)} %dynamic-slice_bitcast_fusion.2, f32[512,2]{0,1:T(2,128)S(1)} %get-tuple-element.270, pred[512,2048]{0,1:T(8,128)(4,1)S(1)} %broadcast_compare_fusion.2), kind=kLoop, calls=%fused_computation.6.clone.1 | loop fusion | flops 12581888 | bytes 9465856 | tf_op jit(solution)/shard_map/while/body/eval_jaxpr/reduce_sum | solution.py:45
  154.6 0.8 copy.35
  155.4 6.4 %fusion.44 = f32[512,2,128]{0,2,1:T(8,128)} fusion(f32[2,2048,512]{2,1,0:T(8,128)} %get-tuple-element.231, f32[512,2]{0,1:T(2,128)S(1)} %fusion.41, f32[2,2048]{1,0:T(2,128)S(1)} %dynamic-slice_bitcast_fusion.2, f32[512,2]{0,1:T(2,128)S(1)} %get-tuple-element.270, pred[512,2048]{0,1:T(8,128)(4,1)S(1)} %broadcast_compare_fusion.2, ...), kind=kOutput, calls=%fused_computation.12.clone.1 | convolution fusion | flops 549847040 | bytes 11563009 | tf_op jit(solution)/shard_map/while/body/eval_jaxpr/qhk,khd->qhd/dot_general | solution.py:46
  161.8 1.1 divide_convert_fusion
  163.1 8.5 %all_to_all.16 = bf16[4,128,256]{2,1,0:T(8,128)(2,1)S(1)} all-to-all(bf16[4,128,256]{2,1,0:T(8,128)(2,1)S(1)} %copy.25), channel_id=1, replica_groups=mesh['sp'=8,'tp'=4] {'tp'}, dimensions={0} | all-to-all | bytes 524288 | tf_op jit(solution)/shard_map/all_to_all | solution.py:58
  171.8 3.2 multiply_reduce_fusion
  175.0 0.9 multiply_convert_fusion.1
  176.8 59.6 %all-gather.15.cloned.1.call-done = bf16[16384,256]{1,0:T(8,128)(2,1)} async-done(((bf16[2048,256]{1,0:T(8,128)(2,1)}), bf16[16384,256]{1,0:T(8,128)(2,1)}) %all-gather.15.cloned.1.call-update) | async-done | bytes 8388624 | tf_op jit(solution)/shard_map/all_gather | solution.py:70
  236.4 11.6 %copy.23 = bf16[2048,8,256]{0,2,1:T(8,128)(2,1)} copy(bf16[2048,8,256]{2,0,1:T(8,128)(2,1)} %bitcast.65) | data formatting | bytes 16777216 | tf_op jit(solution)/shard_map/reshape | solution.py:70
  248.0 10.6 %all-gather.11.cloned.1.call-done = bf16[512,2048]{1,0:T(8,128)(2,1)} async-done(((bf16[128,2048]{1,0:T(8,128)(2,1)}), bf16[512,2048]{1,0:T(8,128)(2,1)}) %all-gather.11.cloned.1.call-update) | async-done | bytes 2097168 | tf_op jit(solution)/shard_map/all_gather | solution.py:63
  258.6 126.5 %all-gather.13.cloned.1.call-done = bf16[2048,2048]{1,0:T(8,128)(2,1)} async-done(((bf16[256,2048]{1,0:T(8,128)(2,1)}), bf16[2048,2048]{1,0:T(8,128)(2,1)}) %all-gather.13.cloned.1.call-update) | async-done | bytes 8388624 | tf_op jit(solution)/shard_map/all_gather | solution.py:66
  385.1 16.5 %convolution_convert_fusion = bf16[512,2048]{1,0:T(8,128)(2,1)} fusion(bf16[2048,2048]{0,1:T(8,128)(2,1)} %bitcast.66, bf16[512,2048]{1,0:T(8,128)(2,1)} %all-gather.11.cloned.1.call-done, bf16[2048,2048]{1,0:T(8,128)(2,1)} %all-gather.13.cloned.1.call-done), kind=kOutput, calls=%fused_computation.30 | convolution fusion | flops 8594128896 | bytes 20971520 | tf_op jit(solution)/shard_map/dot_general | solution.py:71
  401.6 29.5 %reduce-scatter.2.cloned.1.call-done = bf16[128,2048]{1,0:T(8,128)(2,1)} async-done(((bf16[512,2048]{1,0:T(8,128)(2,1)}), bf16[128,2048]{1,0:T(8,128)(2,1)}) %reduce-scatter.2.cloned.1.call-update) | async-done | bytes 524304 | tf_op jit(solution)/shard_map/reduce_scatter | solution.py:72
  431.1 1.9 add_convert_fusion
  (37 shorter events, 5.0 us)
Async XLA Ops:
  6.5 108.6 %copy-start = (f32[512,2]{0,1:T(2,128)S(1)}, f32[512,2]{0,1:T(2,128)}, u32[]{:S(2)}) copy-start(f32[512,2]{0,1:T(2,128)} %param.14) | copy-start | bytes 12292
  6.5 54.9 %all-gather.7.cloned.1.call-start = ((), (), s32[]{:S(2)}) async-start(), calls=%async_computation.2 | async-start | bytes 2359296 | tf_op jit(solution)/shard_map/all_gather | solution.py:23
  7.3 103.9 %all-gather.9.cloned.1.call-start = ((), (), s32[]{:S(2)}) async-start(), calls=%async_computation.3 | async-start | bytes 2359296 | tf_op jit(solution)/shard_map/all_gather | solution.py:24
  8.0 228.4 %all-gather.15.cloned.1.call-start = ((), (), s32[]{:S(2)}) async-start(), calls=%async_computation.7 | async-start | bytes 9437184 | tf_op jit(solution)/shard_map/all_gather | solution.py:70
  8.7 249.8 %all-gather.11.cloned.1.call-start = ((), (), s32[]{:S(2)}) async-start(), calls=%async_computation.4 | async-start | bytes 2621440 | tf_op jit(solution)/shard_map/all_gather | solution.py:63
  161.8 13.2 %copy-start.1 = (f32[2048]{0:T(1024)S(1)}, f32[2048]{0:T(1024)}, u32[]{:S(2)}) copy-start(f32[2048]{0:T(1024)} %param.17) | copy-start | bytes 24580
  176.0 209.1 %all-gather.13.cloned.1.call-start = ((), (), s32[]{:S(2)}) async-start(), calls=%async_computation.5 | async-start | bytes 9437184 | tf_op jit(solution)/shard_map/all_gather | solution.py:66
  176.6 254.5 %reduce-scatter.2.cloned.1.call-start = ((), (), s32[]{:S(2)}) async-start(), calls=%async_computation.6 | async-start | bytes 2621440 | tf_op jit(solution)/shard_map/reduce_scatter | solution.py:72
Sparse Core Ops, SparseCore 0:
  9.5 51.8 all-gather.6
  63.5 47.6 all-gather.8
  113.3 123.0 all-gather.14
  237.8 20.7 all-gather.10
  260.6 124.4 all-gather.12
  401.7 29.3 reduce-scatter.1
